TPU v7x, 32 devices: a whole 2x2x4 slice. The times are simulated.
32 devices in a mesh: fs: 8 (over z, y), tp: 4 (over x, core).
Axes of the slice: x: 2, y: 2, z: 4, core: 2. Of those that a mesh axis runs over, the one named last changes fastest.
Arguments:
- inputs: bfloat16 [4096, 2304], P('fs'), may hold values from -6 to 6
- value_cot: bfloat16 [4096, 4096], P('fs', 'tp'), may hold values from -0.09375 to 0.09375
- retained: bfloat16 [4096, 4096], P('fs', 'tp'), may hold values from -6 to 6
- output_cot: bfloat16 [4096, 2304], P('fs'), may hold values from -0.09375 to 0.09375
- proj_value: bfloat16 [2304, 192], P('fs'), may hold values from -0.125 to 0.125
- proj_output: bfloat16 [2304, 192], P('fs'), may hold values from -0.125 to 0.125
- w_value: float32 [2304, 4096], P('fs', 'tp'), may hold values from -6 to 6
- w_output: float32 [4096, 2304], P('tp', 'fs'), may hold values from -6 to 6
- first_value: float32 [192, 4096], P('fs', 'tp'), may hold values from -106 to 106
- second_value: float32 [192, 4096], P('fs', 'tp'), may hold values from 0.25 to 4
- first_output: float32 [192, 4096], P('fs', 'tp'), may hold values from -106 to 106
- second_output: float32 [192, 4096], P('fs', 'tp'), may hold values from 0.25 to 4
Outputs:
- step_value: float32 [2304, 4096], P('fs', 'tp')
- step_output: float32 [4096, 2304], P('tp', 'fs')
- copy_value: bfloat16 [2304, 4096], P(None, 'tp')
- copy_output: bfloat16 [4096, 2304], P('tp')
- new_first_value: float32 [192, 4096], P('fs', 'tp')
- new_second_value: float32 [192, 4096], P('fs', 'tp')
- new_first_output: float32 [192, 4096], P('fs', 'tp')
- new_second_output: float32 [192, 4096], P('fs', 'tp')
All inputs are finite; a program needn't handle non-finite values.
Results may differ from a plain program's by a relative error of at most 0.0034.
Values may be sent and summed in bfloat16 or wider, within the bound.
A program may use at most 64 MiB of HBM per device.

v0:
```python
import jax
import jax.numpy as jnp
from jax import lax
from jax.sharding import PartitionSpec as P

RANK = 192
HV = 4096


beta_one = 0.8
beta_two = 0.9
moment_eps = 1e-08
norm_eps = 1e-06


def project_rows(inputs, output_cot, pieces):
    return (
        jnp.dot(inputs, pieces[0], preferred_element_type=jnp.float32),
        jnp.dot(output_cot, pieces[1], preferred_element_type=jnp.float32),
    )


def contract_tokens(left, right):
    return lax.dot_general(
        left, right, (((0,), (0,)), ((), ())), preferred_element_type=jnp.float32
    )


def adapt(first, second, grad):
    new_first = beta_one * first + (1.0 - beta_one) * grad
    new_second = beta_two * second + (1.0 - beta_two) * grad * grad
    direction = (new_first / (jnp.sqrt(new_second) + moment_eps)).astype(jnp.bfloat16)
    return (new_first, new_second, direction)


def squares(direction):
    return jnp.sum(jnp.square(direction.astype(jnp.float32)))


def expand(proj_value, proj_output, update_v, update_o, pieces):
    update_v = jnp.dot(proj_value, pieces[0], preferred_element_type=jnp.float32)
    update_o = lax.dot_general(
        pieces[1], proj_output, (((0,), (1,)), ((), ())), preferred_element_type=jnp.float32
    )
    return (update_v, update_o)


def per_device(
    inputs,
    value_cot,
    retained,
    output_cot,
    proj_value,
    proj_output,
    w_value,
    w_output,
    first_value,
    second_value,
    first_output,
    second_output,
):
    folded = project_rows(
        inputs,
        output_cot,
        (
            lax.all_gather(proj_value, "fs", axis=0, tiled=True),
            lax.all_gather(proj_output, "fs", axis=0, tiled=True),
        ),
    )
    x_proj = folded[0].astype(jnp.bfloat16)
    o_proj = folded[1].astype(jnp.bfloat16)
    summed = lax.psum_scatter(
        jnp.concatenate(
            [contract_tokens(x_proj, value_cot), contract_tokens(o_proj, retained)], axis=1
        ),
        "fs",
        scatter_dimension=0,
        tiled=True,
    )
    columns = value_cot.shape[1]
    first_v, second_v, dir_value = adapt(first_value, second_value, summed[:, :columns])
    first_o, second_o, dir_output = adapt(first_output, second_output, summed[:, columns:])
    zero_v = jnp.zeros((proj_value.shape[0], columns), jnp.float32)
    zero_o = jnp.zeros((columns, proj_output.shape[0]), jnp.float32)
    start_state = (zero_v, zero_o, jnp.zeros((), jnp.float32), jnp.zeros((), jnp.float32))
    pieces = (
        lax.all_gather(dir_value, "fs", axis=0, tiled=True),
        lax.all_gather(dir_output, "fs", axis=0, tiled=True),
    )
    update_v, update_o = expand(proj_value, proj_output, start_state[0], start_state[1], pieces)
    totals = lax.psum((squares(pieces[0]), squares(pieces[1])), "tp")
    scale_value = lax.rsqrt(totals[0] / (RANK * HV) + norm_eps)
    scale_output = lax.rsqrt(totals[1] / (RANK * HV) + norm_eps)
    step_value = update_v * scale_value
    step_output = update_o * scale_output
    fresh = (
        (w_value + step_value).astype(jnp.bfloat16),
        (w_output + step_output).astype(jnp.bfloat16),
    )
    copy_value, copy_output = (
        lax.all_gather(fresh[0], "fs", axis=0, tiled=True),
        lax.all_gather(fresh[1], "fs", axis=1, tiled=True),
    )
    return (step_value, step_output, copy_value, copy_output, first_v, second_v, first_o, second_o)


def solution(mesh):
    in_specs = (
        P("fs", None),
        P("fs", "tp"),
        P("fs", "tp"),
        P("fs", None),
        P("fs", None),
        P("fs", None),
        P("fs", "tp"),
        P("tp", "fs"),
        P("fs", "tp"),
        P("fs", "tp"),
        P("fs", "tp"),
        P("fs", "tp"),
    )
    out_specs = (
        P("fs", "tp"),
        P("tp", "fs"),
        P(None, "tp"),
        P("tp", None),
        P("fs", "tp"),
        P("fs", "tp"),
        P("fs", "tp"),
        P("fs", "tp"),
    )
    return jax.shard_map(
        per_device, mesh=mesh, in_specs=in_specs, out_specs=out_specs, check_vma=False
    )
```

profile of v0, /device:TPU:9, one launch (start us, length us, event | category | flops | bytes accessed | tf_op | source)
XLA Modules:
  0.0 404.2 jit_solution(5537055794950769695)
XLA Ops:
  7.2 0.0 copy-start
  7.2 0.0 reduce-scatter.2.cloned.1.call-start
  7.2 0.0 copy-start.2
  7.2 28.9 %all_gather.18 = bf16[2304,192]{1,0:T(8,128)(2,1)} all-gather(bf16[288,192]{1,0:T(8,128)(2,1)} %param.16), channel_id=1, replica_groups=mesh['fs'=8,'tp'=4] {'fs'}, dimensions={0}, use_global_device_ids=true | all-gather | bytes 995328 | tf_op jit(solution)/shard_map/all_gather | solution.py:66
  36.1 0.0 copy-done.2
  36.1 29.7 %all_gather.19 = bf16[2304,192]{1,0:T(8,128)(2,1)S(1)} all-gather(bf16[288,192]{1,0:T(8,128)(2,1)S(1)} %copy-done.2), channel_id=1, replica_groups=mesh['fs'=8,'tp'=4] {'fs'}, dimensions={0}, use_global_device_ids=true | all-gather | bytes 995328 | tf_op jit(solution)/shard_map/all_gather | solution.py:67
  65.9 3.9 fusion.1
  69.8 4.3 %fusion.2 = f32[192,1024]{1,0:T(8,128)} fusion(bf16[512,1024]{1,0:T(8,128)(2,1)} %param.14, bf16[512,2304]{1,0:T(8,128)(2,1)} %param.15, bf16[2304,192]{1,0:T(8,128)(2,1)S(1)} %all_gather.19), kind=kOutput, calls=%fused_computation.9 | convolution fusion | flops 654409728 | bytes 5079040 | tf_op jit(solution)/shard_map/dot_general | solution.py:24
  74.0 2.7 pad_maximum_fusion
  76.7 0.0 reduce-scatter.2.cloned.1.call-update
  76.7 0.0 copy-start.1
  76.8 0.0 all-gather.3.cloned.1.call-start
  76.8 75.2 %reduce-scatter.2.cloned.1.call-done = f32[24,2048]{1,0:T(8,128)} async-done(((f32[192,2048]{1,0:T(8,128)}), f32[24,2048]{1,0:T(8,128)}) %reduce-scatter.2.cloned.1.call-update) | async-done | bytes 196624 | tf_op jit(solution)/shard_map/reduce_scatter | solution.py:72
  152.0 0.0 copy-done.4
  152.0 0.0 copy-done.6
  152.0 1.8 divide_convert_fusion
  153.8 22.4 %all_gather.21 = bf16[192,1024]{1,0:T(8,128)(2,1)S(1)} all-gather(bf16[24,1024]{1,0:T(8,128)(2,1)S(1)} %get-tuple-element.18), channel_id=1, replica_groups=mesh['fs'=8,'tp'=4] {'fs'}, dimensions={0}, use_global_device_ids=true | all-gather | bytes 442368 | tf_op jit(solution)/shard_map/all_gather | solution.py:88
  176.2 0.8 multiply_reduce_fusion
  177.0 24.7 %all_gather.20 = bf16[192,1024]{1,0:T(8,128)(2,1)S(1)} all-gather(bf16[24,1024]{1,0:T(8,128)(2,1)S(1)} %get-tuple-element.24), channel_id=1, replica_groups=mesh['fs'=8,'tp'=4] {'fs'}, dimensions={0}, use_global_device_ids=true | all-gather | bytes 442368 | tf_op jit(solution)/shard_map/all_gather | solution.py:87
  201.8 0.8 multiply_reduce_fusion.1
  202.6 20.9 %all-reduce = (f32[]{:T(128)}, f32[]{:T(128)}) all-reduce(f32[]{:T(128)} %multiply_reduce_fusion.1, f32[]{:T(128)} %multiply_reduce_fusion), channel_id=1, replica_groups=mesh['fs'=8,'tp'=4] {'tp'}, use_global_device_ids=true, to_apply=%region_2.0 | all-reduce | flops 2 | bytes 16 | tf_op jit(solution)/shard_map/psum | solution.py:91
  224.2 0.0 copy-done.1
  224.2 0.0 copy-start.3
  224.2 2.8 add_convert_fusion.1
  227.0 0.0 all-gather.3.cloned.1.call-update
  227.0 0.0 all-gather.5.cloned.1.call-start
  227.8 2.8 add_convert_fusion
  230.6 0.0 all-gather.5.cloned.1.call-update
  230.6 75.0 %all-gather.3.cloned.1.call-done = bf16[2304,1024]{1,0:T(8,128)(2,1)} async-done(((bf16[288,1024]{1,0:T(8,128)(2,1)}), bf16[2304,1024]{1,0:T(8,128)(2,1)}) %all-gather.3.cloned.1.call-update) | async-done | bytes 4718608 | tf_op jit(solution)/shard_map/all_gather | solution.py:101
  305.6 80.5 %all-gather.5.cloned.1.call-done = bf16[1024,2304]{0,1:T(8,128)(2,1)} async-done(((bf16[1024,288]{0,1:T(8,128)(2,1)}), bf16[1024,2304]{0,1:T(8,128)(2,1)}) %all-gather.5.cloned.1.call-update) | async-done | bytes 4718608 | tf_op jit(solution)/shard_map/all_gather | solution.py:102
  386.1 6.6 %copy.20 = bf16[1024,2304]{1,0:T(8,128)(2,1)} copy(bf16[1024,2304]{0,1:T(8,128)(2,1)} %all-gather.5.cloned.1.call-done) | data formatting | bytes 9437184
  392.7 5.0 %copy.22 = bf16[2304,1024]{1,0:T(8,128)(2,1)} copy(bf16[2304,1024]{1,0:T(8,128)(2,1)} %all-gather.3.cloned.1.call-done) | data formatting | bytes 9437184
  (8 shorter events, 0.0 us)
Async XLA Ops:
  7.2 58.7 %copy-start = (bf16[512,2304]{1,0:T(8,128)(2,1)S(1)}, bf16[512,2304]{1,0:T(8,128)(2,1)}, u32[]{:S(2)}) copy-start(bf16[512,2304]{1,0:T(8,128)(2,1)} %param.12) | copy-start | bytes 7077892
  7.2 144.8 %reduce-scatter.2.cloned.1.call-start = ((), (), s32[]{:S(2)}) async-start(), calls=%async_computation.1 | async-start | bytes 1769472 | tf_op jit(solution)/shard_map/reduce_scatter | solution.py:72
  7.2 28.9 %copy-start.2 = (bf16[288,192]{1,0:T(8,128)(2,1)S(1)}, bf16[288,192]{1,0:T(8,128)(2,1)}, u32[]{:S(2)}) copy-start(bf16[288,192]{1,0:T(8,128)(2,1)} %param.17) | copy-start | bytes 331780
  76.7 75.3 %copy-start.4 = (f32[24,1024]{1,0:T(8,128)S(1)}, f32[24,1024]{1,0:T(8,128)}, u32[]{:S(2)}) copy-start(f32[24,1024]{1,0:T(8,128)} %param.23) | copy-start | bytes 294916
  76.7 75.3 %copy-start.5 = (f32[24,1024]{1,0:T(8,128)S(1)}, f32[24,1024]{1,0:T(8,128)}, u32[]{:S(2)}) copy-start(f32[24,1024]{1,0:T(8,128)} %param.22) | copy-start | bytes 294916
  76.7 75.3 %copy-start.6 = (f32[24,1024]{1,0:T(8,128)S(1)}, f32[24,1024]{1,0:T(8,128)}, u32[]{:S(2)}) copy-start(f32[24,1024]{1,0:T(8,128)} %param.21) | copy-start | bytes 294916
  76.7 75.3 %copy-start.7 = (f32[24,1024]{1,0:T(8,128)S(1)}, f32[24,1024]{1,0:T(8,128)}, u32[]{:S(2)}) copy-start(f32[24,1024]{1,0:T(8,128)} %param.20) | copy-start | bytes 294916
  76.7 147.4 %copy-start.1 = (bf16[288,192]{1,0:T(8,128)(2,1)S(1)}, bf16[288,192]{1,0:T(8,128)(2,1)}, u32[]{:S(2)}) copy-start(bf16[288,192]{1,0:T(8,128)(2,1)} %param.16) | copy-start | bytes 331780
  76.8 228.8 %all-gather.3.cloned.1.call-start = ((), (), s32[]{:S(2)}) async-start(), calls=%async_computation.2 | async-start | bytes 5308416 | tf_op jit(solution)/shard_map/all_gather | solution.py:101
  224.2 3.6 copy-start.3
  227.0 159.0 %all-gather.5.cloned.1.call-start = ((), (), s32[]{:S(2)}) async-start(), calls=%async_computation.3 | async-start | bytes 5308416 | tf_op jit(solution)/shard_map/all_gather | solution.py:102
Sparse Core Ops, SparseCore 0:
  76.9 75.0 reduce-scatter.1
  227.1 78.3 all-gather.2
  308.3 77.6 all-gather.4
where the time goes:
time: 409 us; the launch traced here: 404 us
  waiting for transfers between devices  231 us (56%)
  blocking collectives  127 us (31%)
  between operations  15.2 us (4%)
  matrix products  13.8 us (3%)
  local copies, waits for them, and re-layouts  11.7 us (3%)
  other arithmetic  6.02 us (1%)
    all_gather x1, waiting for transfers between devices, per_device(): lax.all_gather(fresh[1], 'fs', axis=1, tiled=True)  80.5 us
    reduce_scatter x1, waiting for transfers between devices, per_device(): lax.psum_scatter(jnp.concatenate([contract_tokens(x_proj, value_cot), con...  75.2 us
    all_gather x1, waiting for transfers between devices, per_device(): lax.all_gather(fresh[0], 'fs', axis=0, tiled=True)  75 us
    all_gather x1, blocking collectives, per_device(): lax.all_gather(proj_output, 'fs', axis=0, tiled=True)  29.7 us
    all_gather x1, blocking collectives, per_device(): lax.all_gather(proj_value, 'fs', axis=0, tiled=True)  28.9 us
    all_gather x1, blocking collectives, per_device(): lax.all_gather(dir_value, 'fs', axis=0, tiled=True)  24.7 us
    all_gather x1, blocking collectives, per_device(): lax.all_gather(dir_output, 'fs', axis=0, tiled=True)  22.4 us
    psum x1, blocking collectives, per_device(): totals = lax.psum((squares(pieces[0]), squares(pieces[1])), 'tp')  20.9 us
  transfers between devices with their start and end apart: 3, of which 3 were waited for; matrix products, arithmetic and copies ran while one was open for 1% of the time, Pallas kernels for 0%

commit v1 on v0

v1 whole, which is shorter than its diff:
```python
import functools

import jax
import jax.numpy as jnp
from jax import lax
from jax.experimental import pallas as pl
from jax.experimental.pallas import tpu as pltpu
from jax.sharding import PartitionSpec as P

BF16 = jnp.bfloat16
F32 = jnp.float32

beta_one = 0.8
beta_two = 0.9
moment_eps = 1e-08
norm_eps = 1e-06

EARLY_NUM, EARLY_DEN = 1, 2


def adapt(first, second, grad):
    new_first = beta_one * first + (1.0 - beta_one) * grad
    new_second = beta_two * second + (1.0 - beta_two) * grad * grad
    direction = (new_first / (jnp.sqrt(new_second) + moment_eps)).astype(BF16)
    return (new_first, new_second, direction)


def flat(block):
    parts, rows, columns = block.shape
    if rows % 16 == 0:
        return block.reshape(parts * rows, columns)
    return block.astype(F32).reshape(parts * rows, columns).astype(block.dtype)


def exchange(
    n, t, x_ref, oc_ref, vc_ref, ret_ref, pv_ref, po_ref, wv_ref, wo_ref, fv_ref, sv_ref, fo_ref, so_ref,
    wall, pall, dall, sq, nfv, nsv, nfo, nso,
    xin, pr, gsend, grecv,
    load_sem, p_send, p_recv, core_send, core_recv, g_send, g_recv, d_send, d_recv, q_send, q_recv,
    ring_send, ring_recv, y_send, y_recv,
):
    me = lax.axis_index("fs")
    tp = lax.axis_index("tp")
    core = lax.rem(tp, 2)
    partner = tp + 1 - 2 * core
    z, y = me // 2, lax.rem(me, 2)
    levels = n // 2
    across = me + 1 - 2 * y
    q, columns = wv_ref.shape
    rows = 2 * q
    early = max(16, (rows * EARLY_NUM // EARLY_DEN) // 16 * 16)
    late = rows - early
    last = levels // 2
    halved = levels % 2 == 0
    rr = fv_ref.shape[0]

    def remote(src, dst, ssem, rsem, device):
        return pltpu.make_async_remote_copy(
            src_ref=src, dst_ref=dst, send_sem=ssem, recv_sem=rsem,
            device_id=device, device_id_type=pl.DeviceIdType.MESH,
        )

    barrier = pltpu.get_barrier_semaphore()
    for d in range(1, n):
        pl.semaphore_signal(
            barrier, inc=1, device_id={"fs": lax.rem(me + d, n)}, device_id_type=pl.DeviceIdType.MESH
        )
    for d in range(1, t):
        pl.semaphore_signal(
            barrier, inc=1, device_id={"tp": lax.rem(tp + d, t)}, device_id_type=pl.DeviceIdType.MESH
        )

    @pl.when(core == 0)
    def _():
        pltpu.make_async_copy(x_ref, xin, load_sem).start()
        pall[0, me] = pv_ref[...]

    @pl.when(core == 1)
    def _():
        pltpu.make_async_copy(oc_ref, xin, load_sem).start()
        pall[1, me] = po_ref[...]

    wall[me, :q] = wv_ref[...].astype(BF16)
    wall[me, q:] = wo_ref[...].astype(BF16)
    pl.semaphore_wait(barrier, n - 1 + t - 1)

    sends = []

    def go(copy):
        copy.start()
        sends.append(copy)
        return copy

    def to_all(buffer, target, ssem, rsem):
        out = []
        for d in range(1, n):
            peer = lax.rem(me + d, n)
            out.append(go(remote(buffer(peer), target, ssem.at[d], rsem.at[d], {"fs": peer})))
        return out

    def span(piece, k, s):
        low, high = (0, late) if piece == 0 else (late, rows)
        if halved and k == last:
            middle = low + (high - low) // 2 // 16 * 16
            low, high = (low, middle) if s == 0 else (middle, high)
        return low, high - low

    def at(level, column, low, size):
        return wall.at[level * 2 + column, pl.ds(low, size)]

    def ring(piece, k, s):
        low, size = span(piece, k, s)
        if size == 0:
            return None
        step = 1 if s == 0 else levels - 1
        level = lax.rem(z + (levels - step) * (k - 1), levels)
        column = y if piece < 2 else 1 - y
        place = at(level, column, low, size)
        target = lax.rem(z + step, levels) * 2 + y
        return go(remote(place, place, ring_send.at[s, k, piece], ring_recv.at[s, k, piece], {"fs": target}))

    def over(k, s):
        low, size = span(0, k, s)
        if size == 0:
            return None
        step = 1 if s == 0 else levels - 1
        level = lax.rem(z + (levels - step) * k, levels)
        place = at(level, y, low, size)
        return go(remote(place, place, y_send.at[s, k], y_recv.at[s, k], {"fs": across}))

    def landed(copy):
        if copy is not None:
            copy.wait_recv()

    proj_copies = to_all(lambda peer: pall.at[core, me], pall.at[core, me], p_send, p_recv)
    own_early = at(z, y, late, early)
    crossed = go(remote(own_early, own_early, y_send.at[1, 0], y_recv.at[1, 0], {"fs": across}))
    steps = {}
    for piece in (0, 1):
        for s in (0, 1):
            steps[piece, 1, s] = ring(piece, 1, s)
    own_late = at(z, y, 0, late)
    overs = [go(remote(own_late, own_late, y_send.at[0, 0], y_recv.at[0, 0], {"fs": across}))]

    for copy in proj_copies:
        copy.wait_recv()
    whole_proj = go(remote(pall.at[core], pall.at[core], core_send.at[0], core_recv.at[0], {"tp": partner}))
    pltpu.make_async_copy(x_ref, xin, load_sem).wait()
    pr[core] = jnp.dot(xin[...], flat(pall[core]), preferred_element_type=F32).astype(BF16)
    swapped = go(remote(pr.at[core], pr.at[core], core_send.at[1], core_recv.at[1], {"tp": partner}))
    swapped.wait_recv()
    for side, cot in ((0, vc_ref), (1, ret_ref)):
        grad = lax.dot_general(
            pr[side], cot[...], (((0,), (0,)), ((), ())), preferred_element_type=F32
        )
        for peer in range(n):
            gsend[peer, :, side * columns:(side + 1) * columns] = (
                grad[peer * rr:(peer + 1) * rr].astype(BF16)
            )
    grad_copies = to_all(lambda peer: gsend.at[peer], grecv.at[me], g_send, g_recv)

    crossed.wait_recv()
    for s in (0, 1):
        steps[2, 1, s] = ring(2, 1, s)

    dir_copies = []
    for k in range(1, last + 1):
        for piece in (0, 1, 2):
            if k == 1 and piece == 2:
                for copy in grad_copies:
                    copy.wait_recv()
                total = gsend[me].astype(F32)
                for d in range(1, n):
                    total += grecv[lax.rem(me + d, n)].astype(F32)
                for side, refs in ((0, (fv_ref, sv_ref, nfv, nsv)), (1, (fo_ref, so_ref, nfo, nso))):
                    part = total[:, side * columns:(side + 1) * columns]
                    new_first, new_second, direction = adapt(refs[0][...], refs[1][...], part)
                    refs[2][...] = new_first
                    refs[3][...] = new_second
                    dall[me, :, side * columns:(side + 1) * columns] = direction
                dir_copies = to_all(lambda peer: dall.at[me], dall.at[me], d_send, d_recv)
            for s in (0, 1):
                landed(steps[piece, k, s])
                if k < last:
                    steps[piece, k + 1, s] = ring(piece, k + 1, s)
                if piece == 0:
                    overs.append(over(k, s))

    for copy in dir_copies:
        copy.wait_recv()
    sums = []
    for side in (0, 1):
        acc = jnp.zeros((rr, columns), F32)
        for k in range(n):
            acc += jnp.square(dall[k, :, side * columns:(side + 1) * columns].astype(F32))
        sums.append(jnp.sum(acc))
    line = lax.broadcasted_iota(jnp.int32, sq.shape[1:], 0)
    sq[tp] = jnp.where(line == 0, sums[0], sums[1])
    sq_copies = []
    for d in range(1, t):
        sq_copies.append(
            go(remote(sq.at[tp], sq.at[tp], q_send.at[d], q_recv.at[d], {"tp": lax.rem(tp + d, t)}))
        )
    for copy in sq_copies:
        copy.wait_recv()
    for copy in overs:
        landed(copy)
    whole_proj.wait_recv()
    for copy in sends:
        copy.wait_send()


def finish(q, count, sq_ref, wall_ref, pall_ref, own_v, own_o, dv_ref, do_ref, step_v, step_o, copy_v, copy_o):
    totals = jnp.sum(sq_ref[...], axis=0)
    scale_v = lax.rsqrt(totals[0:1, 0:1] / count + norm_eps)
    scale_o = lax.rsqrt(totals[1:2, 0:1] / count + norm_eps)
    n, _, lanes = wall_ref.shape
    dir_v, dir_o = dv_ref[...], do_ref[...]
    step_v[...] = jnp.dot(own_v[...], dir_v, preferred_element_type=F32) * scale_v
    step_o[...] = jnp.dot(own_o[...], dir_o, preferred_element_type=F32) * scale_o
    w_v = wall_ref[:, :q].astype(F32).reshape(n * q, lanes)
    w_o = wall_ref[:, q:].astype(F32).reshape(n * q, lanes)
    copy_v[...] = (
        w_v + jnp.dot(pall_ref[0], dir_v, preferred_element_type=F32) * scale_v
    ).astype(BF16)
    moved = w_o + jnp.dot(pall_ref[1], dir_o, preferred_element_type=F32) * scale_o
    copy_o[...] = moved.T.astype(BF16)


def per_device(
    n, t,
    inputs, value_cot, retained, output_cot, proj_value, proj_output, w_value, w_output,
    first_value, second_value, first_output, second_output,
):
    tokens, width = inputs.shape
    q, rank = proj_value.shape
    columns = value_cot.shape[1]
    rr = first_value.shape[0]
    last = n // 2 // 2
    vmem = pl.BlockSpec(memory_space=pltpu.VMEM)
    anywhere = pl.BlockSpec(memory_space=pl.ANY)
    dma = pltpu.SemaphoreType.DMA
    moment = jax.ShapeDtypeStruct((rr, columns), F32)
    wall, pall, dall, sq, first_v, second_v, first_o, second_o = pl.pallas_call(
        functools.partial(exchange, n, t),
        out_shape=(
            jax.ShapeDtypeStruct((n, 2 * q, columns), BF16),
            jax.ShapeDtypeStruct((2, n, q, rank), BF16),
            jax.ShapeDtypeStruct((n, rr, 2 * columns), BF16),
            jax.ShapeDtypeStruct((t, 8, 128), F32),
            moment, moment, moment, moment,
        ),
        in_specs=[anywhere, anywhere] + [vmem] * 10,
        out_specs=(vmem,) * 8,
        scratch_shapes=[
            pltpu.VMEM((tokens, width), BF16),
            pltpu.VMEM((2, tokens, rank), BF16),
            pltpu.VMEM((n, rr, 2 * columns), BF16),
            pltpu.VMEM((n, rr, 2 * columns), BF16),
            dma, dma((n,)), dma((n,)), dma((2,)), dma((2,)), dma((n,)), dma((n,)), dma((n,)), dma((n,)),
            dma((t,)), dma((t,)),
            dma((2, last + 1, 3)), dma((2, last + 1, 3)), dma((2, last + 1)), dma((2, last + 1)),
        ],
        compiler_params=pltpu.CompilerParams(
            collective_id=0, has_side_effects=True, vmem_limit_bytes=60 * 1024 * 1024
        ),
        name="exchange",
    )(
        inputs, output_cot, value_cot, retained, proj_value, proj_output, w_value, w_output.T,
        first_value, second_value, first_output, second_output,
    )
    lanes = 128
    tiles = columns // lanes
    dirs = dall.reshape(n * rr, 2 * columns)
    full = n * q
    step_v, step_o, copy_v, copy_o = pl.pallas_call(
        functools.partial(finish, q, float(rank * columns * t)),
        grid=(tiles,),
        out_shape=(
            jax.ShapeDtypeStruct((q, columns), F32),
            jax.ShapeDtypeStruct((q, columns), F32),
            jax.ShapeDtypeStruct((full, columns), BF16),
            jax.ShapeDtypeStruct((columns, full), BF16),
        ),
        in_specs=[
            pl.BlockSpec((t, 8, 128), lambda j: (0, 0, 0)),
            pl.BlockSpec((n, 2 * q, lanes), lambda j: (0, 0, j)),
            pl.BlockSpec((2, full, rank), lambda j: (0, 0, 0)),
            pl.BlockSpec((q, rank), lambda j: (0, 0)),
            pl.BlockSpec((q, rank), lambda j: (0, 0)),
            pl.BlockSpec((rank, lanes), lambda j: (0, j)),
            pl.BlockSpec((rank, lanes), lambda j: (0, j + tiles)),
        ],
        out_specs=(
            pl.BlockSpec((q, lanes), lambda j: (0, j)),
            pl.BlockSpec((q, lanes), lambda j: (0, j)),
            pl.BlockSpec((full, lanes), lambda j: (0, j)),
            pl.BlockSpec((lanes, full), lambda j: (j, 0)),
        ),
        compiler_params=pltpu.CompilerParams(vmem_limit_bytes=48 * 1024 * 1024),
        name="finish",
    )(sq, wall, pall.reshape(2, full, rank), proj_value, proj_output, dirs, dirs)
    return (step_v, step_o.T, copy_v, copy_o, first_v, second_v, first_o, second_o)


def solution(mesh):
    in_specs = (
        P("fs", None),
        P("fs", "tp"),
        P("fs", "tp"),
        P("fs", None),
        P("fs", None),
        P("fs", None),
        P("fs", "tp"),
        P("tp", "fs"),
        P("fs", "tp"),
        P("fs", "tp"),
        P("fs", "tp"),
        P("fs", "tp"),
    )
    out_specs = (
        P("fs", "tp"),
        P("tp", "fs"),
        P(None, "tp"),
        P("tp", None),
        P("fs", "tp"),
        P("fs", "tp"),
        P("fs", "tp"),
        P("fs", "tp"),
    )
    return jax.shard_map(
        functools.partial(per_device, mesh.shape["fs"], mesh.shape["tp"]),
        mesh=mesh, in_specs=in_specs, out_specs=out_specs, check_vma=False,
    )
```

time: 409 us -> 209 us (0.51)
  waiting for transfers between devices: 231 us -> 0 us
  Pallas kernels: 0 us -> 201 us
  blocking collectives: 127 us -> 0 us
  between operations: 15.2 us -> 0.7 us
  matrix products: 13.8 us -> 0 us
  other arithmetic: 6.02 us -> 0 us
  local copies, waits for them, and re-layouts: 11.7 us -> 6.09 us
    pallas_call x0 -> x2, Pallas kernels: none -> 201 us  [the longest x1 189 us: per_device(): pl.pallas_call(functools.partial(exchange, n, t), out_shape=(jax.ShapeDty...]
    all_gather x2 -> x0, waiting for transfers between devices: 155 us -> none  [the longest x1 80.5 us: per_device(): lax.all_gather(fresh[1], 'fs', axis=1, tiled=True)]
    all_gather x4 -> x0, blocking collectives: 106 us -> none  [the longest x1 29.7 us: per_device(): lax.all_gather(proj_output, 'fs', axis=0, tiled=True)]
    reduce_scatter x1 -> x0, waiting for transfers between devices: 75.2 us -> none  [per_device(): lax.psum_scatter(jnp.concatenate([contract_tokens(x_proj, value_cot), con...]
    psum x1 -> x0, blocking collectives: 20.9 us -> none  [per_device(): totals = lax.psum((squares(pieces[0]), squares(pieces[1])), 'tp')]
    dot_general x4 -> x0, matrix products: 13.8 us -> none  [the longest x2 8.19 us: contract_tokens(): lax.dot_general(left, right, (((0,), (0,)), ((), ())), preferred_element_...]
    unnamed x18 -> x22, local copies, waits for them, and re-layouts: 11.7 us -> 6.09 us
  transfers between devices with their start and end apart: 3 -> 0, of which waited for: 3 -> 0; matrix products, arithmetic and copies ran while one was open for 1% -> 0% of each run, Pallas kernels for 0% -> 0%
where the time goes in v1:
time: 209 us; the launch traced here: 208 us
  Pallas kernels  201 us (96%)
  local copies, waits for them, and re-layouts  6.09 us (3%)
    pallas_call x1, Pallas kernels, per_device(): pl.pallas_call(functools.partial(exchange, n, t), out_shape=(jax.ShapeDty...  189 us
    pallas_call x1, Pallas kernels, per_device(): pl.pallas_call(functools.partial(finish, q, float(rank * columns * t)), g...  12.2 us
    unnamed x22, local copies, waits for them, and re-layouts  6.09 us

profile of v1, /device:TPU:9, one launch (start us, length us, event | category | flops | bytes accessed | tf_op | source)
XLA Modules:
  0.0 208.2 jit_solution(17360138090316310859)
XLA Ops:
  0.6 0.0 copy-start.2
  0.6 0.0 copy-start.3
  0.7 189.2 %exchange.1 = (bf16[8,576,1024]{2,1,0:T(8,128)(2,1)}, bf16[2,8,288,192]{3,2,1,0:T(8,128)(2,1)}, bf16[8,24,2048]{2,1,0:T(8,128)(2,1)}, f32[4,8,128]{2,1,0:T(8,128...) custom-call(bf16[512,2304]{1,0:T(8,128)(2,1)} %x_ref.1, ...), custom_call_target="tpu_custom_call" | custom-call | tf_op jit(solution)/shard_map/exchange/pallas_call | solution.py:244
  189.9 0.0 copy-done.2
  189.9 0.0 copy-done.3
  189.9 0.0 copy-start
  189.9 1.1 copy-done
  191.1 0.0 copy-start.1
  191.1 1.7 copy-done.1
  192.7 0.0 copy-start.4
  192.7 0.7 copy-done.4
  193.4 0.0 copy-start.8
  193.4 0.0 copy-start.7
  193.5 0.0 copy-start.6
  193.5 0.0 copy-start.5
  193.5 12.2 %finish.1 = (f32[288,1024]{1,0:T(8,128)}, f32[288,1024]{1,0:T(8,128)}, bf16[2304,1024]{1,0:T(8,128)(2,1)}, bf16[1024,2304]{1,0:T(8,128)(2,1)}) custom-call(f32[4,8,128]{2,1,0:T(8,128)S(1)} %copy-done.4, bf16[8,576,1024]{2,1,0:T(8,128)(2,1)} %get-tuple-element.21.wall_ref, bf16[2,2304,192]{2,1,0:T(8,128)(2,1)S(1)} %bitcast.6, bf16[288,192]{1,0:T(8,128)(2,1)S(1)} %copy-done.2, ...), custom_call_target="tpu_custom_call" | custom-call | tf_op jit(solution)/shard_map/finish/pallas_call | solution.py:276
  205.6 0.0 copy-done.8
  205.6 0.6 copy.24
  206.3 0.0 copy-done.7
  206.3 0.6 copy.25
  206.9 0.0 copy-done.6
  206.9 0.6 copy.26
  207.6 0.0 copy-done.5
  207.6 0.6 copy.27
Async XLA Ops:
  0.6 189.3 %copy-start.2 = (bf16[288,192]{1,0:T(8,128)(2,1)S(1)}, bf16[288,192]{1,0:T(8,128)(2,1)}, u32[]{:S(2)}) copy-start(bf16[288,192]{1,0:T(8,128)(2,1)} %own_v.1) | copy-start | bytes 331780
  0.6 189.3 %copy-start.3 = (bf16[288,192]{1,0:T(8,128)(2,1)S(1)}, bf16[288,192]{1,0:T(8,128)(2,1)}, u32[]{:S(2)}) copy-start(bf16[288,192]{1,0:T(8,128)(2,1)} %own_o.1) | copy-start | bytes 331780
  189.9 1.1 copy-start
  191.1 1.7 copy-start.1
  192.7 0.7 copy-start.4
  193.4 12.2 %copy-start.8 = (f32[24,1024]{1,0:T(8,128)S(1)}, f32[24,1024]{1,0:T(8,128)}, u32[]{:S(2)}) copy-start(f32[24,1024]{1,0:T(8,128)} %get-tuple-element.44) | copy-start | bytes 294916
  193.4 12.8 %copy-start.7 = (f32[24,1024]{1,0:T(8,128)S(1)}, f32[24,1024]{1,0:T(8,128)}, u32[]{:S(2)}) copy-start(f32[24,1024]{1,0:T(8,128)} %get-tuple-element.45) | copy-start | bytes 294916
  193.5 13.5 %copy-start.6 = (f32[24,1024]{1,0:T(8,128)S(1)}, f32[24,1024]{1,0:T(8,128)}, u32[]{:S(2)}) copy-start(f32[24,1024]{1,0:T(8,128)} %get-tuple-element.46) | copy-start | bytes 294916
  193.5 14.1 %copy-start.5 = (f32[24,1024]{1,0:T(8,128)S(1)}, f32[24,1024]{1,0:T(8,128)}, u32[]{:S(2)}) copy-start(f32[24,1024]{1,0:T(8,128)} %get-tuple-element.47) | copy-start | bytes 294916

commit v2 on v1

--- a/solution.py
+++ b/solution.py
@@ -15,7 +15,8 @@
 moment_eps = 1e-08
 norm_eps = 1e-06
 
-EARLY_NUM, EARLY_DEN = 1, 2
+EARLY_NUM, EARLY_DEN = 1, 6
+CHUNKS = 4
 
 
 def adapt(first, second, grad):
@@ -98,8 +99,29 @@
             out.append(go(remote(buffer(peer), target, ssem.at[d], rsem.at[d], {"fs": peer})))
         return out
 
+    def spread(place, ssem, rsem):
+        own = place(me)
+        first = [go(remote(own, own, ssem.at[0], rsem.at[0], {"fs": across}))]
+        for d in range(1, levels):
+            target = lax.rem(z + d, levels) * 2 + y
+            first.append(go(remote(own, own, ssem.at[d], rsem.at[d], {"fs": target})))
+        return first
+
+    def pass_on(first, place, ssem, rsem):
+        second = []
+        for d in range(1, levels):
+            first[d].wait_recv()
+            block = place(lax.rem(z + levels - d, levels) * 2 + y)
+            second.append(
+                go(remote(block, block, ssem.at[levels + d], rsem.at[levels + d], {"fs": across}))
+            )
+        return first[:1] + second
+
+    def edge(piece):
+        return late if piece == CHUNKS else late * piece // CHUNKS // 16 * 16
+
     def span(piece, k, s):
-        low, high = (0, late) if piece == 0 else (late, rows)
+        low, high = (edge(piece), edge(piece + 1)) if piece < CHUNKS else (late, rows)
         if halved and k == last:
             middle = low + (high - low) // 2 // 16 * 16
             low, high = (low, middle) if s == 0 else (middle, high)
@@ -114,33 +136,33 @@
             return None
         step = 1 if s == 0 else levels - 1
         level = lax.rem(z + (levels - step) * (k - 1), levels)
-        column = y if piece < 2 else 1 - y
+        column = y if piece <= CHUNKS else 1 - y
         place = at(level, column, low, size)
         target = lax.rem(z + step, levels) * 2 + y
         return go(remote(place, place, ring_send.at[s, k, piece], ring_recv.at[s, k, piece], {"fs": target}))
 
-    def over(k, s):
-        low, size = span(0, k, s)
+    def over(piece, k, s):
+        low, size = span(piece, k, s)
         if size == 0:
             return None
         step = 1 if s == 0 else levels - 1
         level = lax.rem(z + (levels - step) * k, levels)
         place = at(level, y, low, size)
-        return go(remote(place, place, y_send.at[s, k], y_recv.at[s, k], {"fs": across}))
+        return go(remote(place, place, y_send.at[s, k, piece], y_recv.at[s, k, piece], {"fs": across}))
 
     def landed(copy):
         if copy is not None:
             copy.wait_recv()
 
-    proj_copies = to_all(lambda peer: pall.at[core, me], pall.at[core, me], p_send, p_recv)
+    proj_first = spread(lambda block: pall.at[core, block], p_send, p_recv)
     own_early = at(z, y, late, early)
-    crossed = go(remote(own_early, own_early, y_send.at[1, 0], y_recv.at[1, 0], {"fs": across}))
+    crossed = go(remote(own_early, own_early, y_send.at[1, 0, 0], y_recv.at[1, 0, 0], {"fs": across}))
     steps = {}
-    for piece in (0, 1):
+    for piece in range(CHUNKS + 1):
         for s in (0, 1):
             steps[piece, 1, s] = ring(piece, 1, s)
-    own_late = at(z, y, 0, late)
-    overs = [go(remote(own_late, own_late, y_send.at[0, 0], y_recv.at[0, 0], {"fs": across}))]
+    proj_copies = pass_on(proj_first, lambda block: pall.at[core, block], p_send, p_recv)
+    overs = [over(piece, 0, 0) for piece in range(CHUNKS)]
 
     for copy in proj_copies:
         copy.wait_recv()
@@ -161,12 +183,11 @@
 
     crossed.wait_recv()
     for s in (0, 1):
-        steps[2, 1, s] = ring(2, 1, s)
-
-    dir_copies = []
+        steps[CHUNKS + 1, 1, s] = ring(CHUNKS + 1, 1, s)
+
     for k in range(1, last + 1):
-        for piece in (0, 1, 2):
-            if k == 1 and piece == 2:
+        for piece in range(CHUNKS + 2):
+            if k == 1 and piece == CHUNKS + 1:
                 for copy in grad_copies:
                     copy.wait_recv()
                 total = gsend[me].astype(F32)
@@ -178,15 +199,15 @@
                     refs[2][...] = new_first
                     refs[3][...] = new_second
                     dall[me, :, side * columns:(side + 1) * columns] = direction
-                dir_copies = to_all(lambda peer: dall.at[me], dall.at[me], d_send, d_recv)
+                dir_first = spread(lambda block: dall.at[block], d_send, d_recv)
             for s in (0, 1):
                 landed(steps[piece, k, s])
                 if k < last:
                     steps[piece, k + 1, s] = ring(piece, k + 1, s)
-                if piece == 0:
-                    overs.append(over(k, s))
-
-    for copy in dir_copies:
+                if piece < CHUNKS:
+                    overs.append(over(piece, k, s))
+
+    for copy in pass_on(dir_first, lambda block: dall.at[block], d_send, d_recv):
         copy.wait_recv()
     sums = []
     for side in (0, 1):
@@ -259,7 +280,8 @@
             pltpu.VMEM((n, rr, 2 * columns), BF16),
             dma, dma((n,)), dma((n,)), dma((2,)), dma((2,)), dma((n,)), dma((n,)), dma((n,)), dma((n,)),
             dma((t,)), dma((t,)),
-            dma((2, last + 1, 3)), dma((2, last + 1, 3)), dma((2, last + 1)), dma((2, last + 1)),
+            dma((2, last + 1, CHUNKS + 2)), dma((2, last + 1, CHUNKS + 2)),
+            dma((2, last + 1, CHUNKS)), dma((2, last + 1, CHUNKS)),
         ],
         compiler_params=pltpu.CompilerParams(
             collective_id=0, has_side_effects=True, vmem_limit_bytes=60 * 1024 * 1024

time: 209 us -> 171 us (0.82)
  Pallas kernels: 201 us -> 163 us
    pallas_call x1, Pallas kernels: 189 us -> 151 us  [per_device(): pl.pallas_call(functools.partial(exchange, n, t), out_shape=(jax.ShapeDty...]
where the time goes in v2:
time: 171 us; the launch traced here: 170 us
  Pallas kernels  163 us (95%)
  local copies, waits for them, and re-layouts  6.09 us (4%)
    pallas_call x1, Pallas kernels, per_device(): pl.pallas_call(functools.partial(exchange, n, t), out_shape=(jax.ShapeDty...  151 us
    pallas_call x1, Pallas kernels, per_device(): pl.pallas_call(functools.partial(finish, q, float(rank * columns * t)), g...  12.2 us
    unnamed x22, local copies, waits for them, and re-layouts  6.09 us

profile of v2, /device:TPU:9, one launch (start us, length us, event | category | flops | bytes accessed | tf_op | source)
XLA Modules:
  0.0 169.7 jit_solution(3161248524397637789)
XLA Ops:
  0.6 0.0 copy-start.2
  0.6 0.0 copy-start.3
  0.7 150.8 %exchange.1 = (bf16[8,576,1024]{2,1,0:T(8,128)(2,1)}, bf16[2,8,288,192]{3,2,1,0:T(8,128)(2,1)}, bf16[8,24,2048]{2,1,0:T(8,128)(2,1)}, f32[4,8,128]{2,1,0:T(8,128...) custom-call(bf16[512,2304]{1,0:T(8,128)(2,1)} %x_ref.1, ...), custom_call_target="tpu_custom_call" | custom-call | tf_op jit(solution)/shard_map/exchange/pallas_call | solution.py:265
  151.4 0.0 copy-done.2
  151.4 0.0 copy-done.3
  151.5 0.0 copy-start
  151.5 1.1 copy-done
  152.6 0.0 copy-start.1
  152.6 1.7 copy-done.1
  154.3 0.0 copy-start.4
  154.3 0.7 copy-done.4
  155.0 0.0 copy-start.8
  155.0 0.0 copy-start.7
  155.0 0.0 copy-start.6
  155.0 0.0 copy-start.5
  155.0 12.2 %finish.1 = (f32[288,1024]{1,0:T(8,128)}, f32[288,1024]{1,0:T(8,128)}, bf16[2304,1024]{1,0:T(8,128)(2,1)}, bf16[1024,2304]{1,0:T(8,128)(2,1)}) custom-call(f32[4,8,128]{2,1,0:T(8,128)S(1)} %copy-done.4, bf16[8,576,1024]{2,1,0:T(8,128)(2,1)} %get-tuple-element.21.wall_ref, bf16[2,2304,192]{2,1,0:T(8,128)(2,1)S(1)} %bitcast.6, bf16[288,192]{1,0:T(8,128)(2,1)S(1)} %copy-done.2, ...), custom_call_target="tpu_custom_call" | custom-call | tf_op jit(solution)/shard_map/finish/pallas_call | solution.py:298
  167.2 0.0 copy-done.8
  167.2 0.6 copy.24
  167.8 0.0 copy-done.7
  167.8 0.6 copy.25
  168.4 0.0 copy-done.6
  168.4 0.6 copy.26
  169.1 0.0 copy-done.5
  169.1 0.6 copy.27
Async XLA Ops:
  0.6 150.8 %copy-start.2 = (bf16[288,192]{1,0:T(8,128)(2,1)S(1)}, bf16[288,192]{1,0:T(8,128)(2,1)}, u32[]{:S(2)}) copy-start(bf16[288,192]{1,0:T(8,128)(2,1)} %own_v.1) | copy-start | bytes 331780
  0.6 150.8 %copy-start.3 = (bf16[288,192]{1,0:T(8,128)(2,1)S(1)}, bf16[288,192]{1,0:T(8,128)(2,1)}, u32[]{:S(2)}) copy-start(bf16[288,192]{1,0:T(8,128)(2,1)} %own_o.1) | copy-start | bytes 331780
  151.5 1.1 copy-start
  152.6 1.7 copy-start.1
  154.3 0.7 copy-start.4
  155.0 12.2 %copy-start.8 = (f32[24,1024]{1,0:T(8,128)S(1)}, f32[24,1024]{1,0:T(8,128)}, u32[]{:S(2)}) copy-start(f32[24,1024]{1,0:T(8,128)} %get-tuple-element.44) | copy-start | bytes 294916
  155.0 12.8 %copy-start.7 = (f32[24,1024]{1,0:T(8,128)S(1)}, f32[24,1024]{1,0:T(8,128)}, u32[]{:S(2)}) copy-start(f32[24,1024]{1,0:T(8,128)} %get-tuple-element.45) | copy-start | bytes 294916
  155.0 13.5 %copy-start.6 = (f32[24,1024]{1,0:T(8,128)S(1)}, f32[24,1024]{1,0:T(8,128)}, u32[]{:S(2)}) copy-start(f32[24,1024]{1,0:T(8,128)} %get-tuple-element.46) | copy-start | bytes 294916
  155.0 14.1 %copy-start.5 = (f32[24,1024]{1,0:T(8,128)S(1)}, f32[24,1024]{1,0:T(8,128)}, u32[]{:S(2)}) copy-start(f32[24,1024]{1,0:T(8,128)} %get-tuple-element.47) | copy-start | bytes 294916
